TPU v7x, 512 devices: a whole 4x4x16 slice. The times are simulated.
512 devices in a mesh: dp: 4 (over x), kv: 64 (over z, y), tp: 2 (over core).
Axes of the slice: x: 4, y: 4, z: 16, core: 2. Of those that a mesh axis runs over, the one named last changes fastest.
Arguments:
- tokens: bfloat16 [65536, 4096], P(('dp', 'kv')), parts along dimension 0, may hold values from -16 to 16
- query_weight: bfloat16 [4096, 1024], P('kv', 'tp'), may hold values from -0.09375 to 0.09375
- key_weight: bfloat16 [4096, 256], P('kv', 'tp'), may hold values from -0.09375 to 0.09375
- value_weight: bfloat16 [4096, 256], P('kv', 'tp'), may hold values from -0.09375 to 0.09375
- out_weight: bfloat16 [1024, 4096], P('kv', 'tp'), may hold values from -1.5 to 1.5
- chosen: int32 [2048, 16], P(('dp', 'kv')), parts along dimension 0, may hold values from -1 to 511, as said below
- live_length: int32 [4], P('dp'), parts along dimension 0, may hold values from 2048 to 16384
Outputs:
- mixed: bfloat16 [65536, 4096], P(('dp', 'kv'), 'tp'), parts along dimension 0
There are 4 independent parts, one for each index of `dp`. A program takes and returns all parts, laid end to end along the dimension named above; an argument that names none is the same for every part. Nothing has to cross between parts.
Inputs may be any that keep to these rules, and one draw needn't show every extreme that they name: `chosen`: row j lists 16 entries: entry 0 is j itself, the others are distinct blocks before j, or -1 for unused entries. The query blocks of one device together read at most 2 distinct blocks held by any one other device, and some device reads 2 of another's in every draw.
All inputs are finite; a program needn't handle non-finite values.
Results may differ from a plain program's by a relative error of at most 0.0085.
Values may be sent and summed in bfloat16 or wider, within the bound.
No kernel may reach another device: no remote copies, remote signals or barrier semaphores. Data moves between devices by JAX's collectives and lax.ppermute only.
A program may use at most 64 MiB of HBM per device.

v0:
```python
import jax
import jax.numpy as jnp
from jax import lax
from jax.sharding import Mesh
from jax.sharding import PartitionSpec as P

HD = 128
BLOCK = 32
CAP = 2
KV = ("kv_0", "kv_1")
DP_KV = ("dp", "kv_0", "kv_1")


def copy_for_each(shard, axis):
    count = lax.axis_size(axis)
    return lax.all_to_all(
        jnp.broadcast_to(shard[None], (count, *shard.shape)), axis, 0, 0, tiled=True
    )


def laid_out(blocks, dim):
    lengths = list(blocks.shape[1:])
    lengths[dim] *= blocks.shape[0]
    return jnp.moveaxis(blocks, 0, dim).reshape(lengths)


def gathered_copies(shard, axis, dim):
    blocks = copy_for_each(shard, axis)
    return laid_out(blocks, dim)


def spread_rows(shard):
    planes = lax.axis_size("dp")
    rows = shard.shape[0] // planes
    mine = lax.dynamic_slice_in_dim(shard, lax.axis_index("dp") * rows, rows, axis=0)
    column = copy_for_each(mine, "kv_0")
    every = copy_for_each(column, ("dp", "kv_1"))
    tall, wide = (column.shape[0], lax.axis_size("kv_1"))
    every = every.reshape(planes, wide, tall, rows, -1)
    return jnp.transpose(every, (2, 1, 0, 3, 4)).reshape(tall * wide * planes * rows, -1)


def body(tokens, query_weight, key_weight, value_weight, out_weight, chosen, live_length):
    rows = tokens.shape[0]
    per_dev = rows // BLOCK
    owners = lax.axis_size(KV)
    me = lax.axis_index(KV)

    def add_rows(piece):
        return jnp.dot(tokens, piece, preferred_element_type=jnp.float32)

    paired = add_rows(spread_rows(jnp.concatenate([key_weight, value_weight], axis=1))).astype(
        jnp.bfloat16
    )
    queries = add_rows(lax.all_gather(query_weight, KV, axis=0, tiled=True)).astype(jnp.bfloat16)
    width = paired.shape[1]
    local_blocks = paired.reshape(per_dev, BLOCK, width)
    valid = chosen >= 0
    safe = jnp.maximum(chosen, 0)
    blocks_all = owners * per_dev
    hits = (safe[:, :, None] == jnp.arange(blocks_all, dtype=jnp.int32)[None, None, :]) & valid[
        :, :, None
    ]
    needed = jnp.any(hits, axis=(0, 1)).reshape(owners, per_dev)
    needed = needed & (jnp.arange(owners, dtype=jnp.int32) != me)[:, None]
    ranks = jnp.cumsum(needed.astype(jnp.int32), axis=1)
    local_ids = jnp.arange(per_dev, dtype=jnp.int32)
    slot_lists = []
    for slot in range(CAP):
        marked = needed & (ranks == slot + 1)
        found = jnp.any(marked, axis=1)
        where_at = jnp.sum(jnp.where(marked, local_ids[None, :], 0), axis=1)
        slot_lists.append(jnp.where(found, where_at, -1))
    wanted = jnp.stack(slot_lists, axis=1)
    requested = lax.all_to_all(wanted, KV, split_axis=0, concat_axis=0, tiled=True)
    outgoing = local_blocks[jnp.maximum(requested, 0)]
    outgoing = jnp.where((requested >= 0)[:, :, None, None], outgoing, jnp.zeros((), jnp.bfloat16))
    incoming = lax.all_to_all(outgoing, KV, split_axis=0, concat_axis=0, tiled=True)
    table = jnp.concatenate([incoming.reshape(owners * CAP, BLOCK, width), local_blocks], axis=0)
    segment_retainer = safe // per_dev
    local_of = safe % per_dev
    match = (wanted[None, None, :, :] == local_of[:, :, None, None]) & (
        jnp.arange(owners, dtype=jnp.int32)[None, None, :, None]
        == segment_retainer[:, :, None, None]
    )
    slot_index = jnp.arange(owners * CAP, dtype=jnp.int32).reshape(owners, CAP)
    remote_at = jnp.sum(jnp.where(match, slot_index[None, None], 0), axis=(2, 3))
    position = jnp.where(segment_retainer == me, owners * CAP + local_of, remote_at)
    picked = table[position]
    near_keys = picked[..., :HD]
    near_values = picked[..., HD:]
    grouped = queries.reshape(per_dev, BLOCK, -1, HD)
    scores = jnp.einsum(
        "jqhd,jnbd->jhqnb", grouped, near_keys, preferred_element_type=jnp.float32
    ) * HD ** (-0.5)
    query_pos = (me * per_dev + jnp.arange(per_dev, dtype=jnp.int32))[:, None] * BLOCK + jnp.arange(
        BLOCK, dtype=jnp.int32
    )[None, :]
    key_pos = safe[:, :, None] * BLOCK + jnp.arange(BLOCK, dtype=jnp.int32)[None, None, :]
    allowed = valid[:, None, :, None] & (key_pos[:, None, :, :] <= query_pos[:, :, None, None])
    masked = jnp.where(allowed[:, None], scores, -jnp.inf)
    top = jnp.max(masked, axis=(3, 4), keepdims=True)
    weights = jnp.exp(masked - top)
    total = jnp.sum(weights, axis=(3, 4))
    summed = jnp.einsum(
        "jhqnb,jnbd->jqhd",
        weights.astype(jnp.bfloat16),
        near_values,
        preferred_element_type=jnp.float32,
    )
    result = summed / jnp.transpose(total, (0, 2, 1))[..., None]
    live = query_pos < live_length[0]
    result = jnp.where(live[:, :, None, None], result, 0.0)
    attended = result.astype(jnp.bfloat16).reshape(rows, -1)
    every_head = gathered_copies(attended, "tp", 1)
    mixed = jnp.dot(
        every_head,
        lax.all_gather(out_weight, KV, axis=0, tiled=True),
        preferred_element_type=jnp.float32,
    )
    return mixed.astype(jnp.bfloat16)


def solution(mesh):
    split = Mesh(
        mesh.devices.reshape(mesh.shape["dp"], 16, 4, mesh.shape["tp"]),
        ("dp", "kv_0", "kv_1", "tp"),
    )
    placed = (
        P(DP_KV, None),
        P(KV, "tp"),
        P(KV, "tp"),
        P(KV, "tp"),
        P(KV, "tp"),
        P(DP_KV, None),
        P("dp"),
    )
    return jax.shard_map(
        body, mesh=split, in_specs=placed, out_specs=P(DP_KV, "tp"), check_vma=False
    )
```

profile of v0, /device:TPU:2, one launch (start us, length us, event | category | flops | bytes accessed | tf_op | source)
XLA Modules:
  0.0 375.7 jit_solution(15250901952565097661)
XLA Ops:
  6.5 0.0 copy-start
  6.5 0.0 all-gather.3.cloned.1.call-start
  6.5 0.7 all-gather.3.cloned.1.call-update
  7.3 0.7 broadcast_compare_fusion.1
  8.0 0.7 add_select_fusion.1
  8.7 0.1 fusion.21
  8.8 0.1 reshape.152
  8.9 0.1 and_convert_fusion
  9.0 0.2 reduce_window_sum.11
  9.1 0.2 select_reduce_fusion.2
  9.3 0.1 reduce_or.28
  9.4 0.1 reduce_or.29
  9.6 0.7 copy.37
  10.3 18.7 %all-to-all-start = ((s32[64,1,2]{2,1,0:T(1,128)}), s32[64,1,2]{2,1,0:T(1,128)S(1)}, u32[]{:S(2)}, u32[]{:S(2)}) async-start(s32[64,1,2]{2,1,0:T(1,128)} %copy.37), calls=%async_computation | async-start | bytes 65536 | tf_op jit(solution)/shard_map/all_to_all | solution.py:75
  29.1 0.7 fusion.22
  29.8 13.8 %all-to-all-done = s32[64,1,2]{2,1,0:T(1,128)S(1)} async-done(((s32[64,1,2]{2,1,0:T(1,128)}), s32[64,1,2]{2,1,0:T(1,128)S(1)}, u32[]{:S(2)}, u32[]{:S(2)}) %all-to-all-start) | async-done | bytes 544 | tf_op jit(solution)/shard_map/all_to_all | solution.py:75
  43.6 16.8 %all_to_all.29 = bf16[16,16,256]{2,1,0:T(8,128)(2,1)S(1)} all-to-all(bf16[16,16,256]{2,1,0:T(8,128)(2,1)S(1)} %broadcast_in_dim.122), channel_id=1, replica_groups=mesh['dp'=4,'kv_0'=16,'kv_1'=4,'tp'=2] {'kv_0'}, dimensions={0} | all-to-all | bytes 262144 | tf_op jit(solution)/shard_map/all_to_all | solution.py:16
  60.4 1.5 broadcast_in_dim.123
  61.9 5.4 %all-to-all-start.2 = ((bf16[16,16,16,256]{3,2,1,0:T(8,128)(2,1)}), bf16[16,16,16,256]{3,2,1,0:T(8,128)(2,1)}, u32[]{:S(2)}, u32[]{:S(2)}) async-start(bf16[16,16,16,256]{3,2,1,0:T(8,128)(2,1)} %broadcast_in_dim.123), calls=%async_computation.2 | async-start | bytes 4194304 | tf_op jit(solution)/shard_map/all_to_all | solution.py:16
  67.3 0.1 maximum_reduce_fusion
  67.4 0.1 reshape.161
  67.6 0.1 copy.38
  67.7 0.1 copy.39
  67.9 24.0 %all-to-all-done.2 = bf16[16,16,16,256]{3,2,1,0:T(8,128)(2,1)} async-done(((bf16[16,16,16,256]{3,2,1,0:T(8,128)(2,1)}), bf16[16,16,16,256]{3,2,1,0:T(8,128)(2,1)}, u32[]{:S(2)}, u32[]{:S(2)}) %all-to-all-start.2) | async-done | bytes 2097184 | tf_op jit(solution)/shard_map/all_to_all | solution.py:16
  91.9 1.9 copy.40
  93.7 0.0 copy-done
  93.8 0.7 convolution_convert_fusion.2
  94.5 2.0 gather_fusion
  96.5 3.1 broadcast_select_fusion
  99.6 0.0 copy-start.2
  99.6 8.6 %all-to-all-start.3 = ((bf16[64,2,32,256]{3,2,1,0:T(8,128)(2,1)}), bf16[64,2,32,256]{3,2,1,0:T(8,128)(2,1)}, u32[]{:S(2)}, u32[]{:S(2)}) async-start(bf16[64,2,32,256]{3,2,1,0:T(8,128)(2,1)} %broadcast_select_fusion), calls=%async_computation.3 | async-start | bytes 4194304 | tf_op jit(solution)/shard_map/all_to_all | solution.py:78
  108.2 0.0 all-gather.5.cloned.1.call-start
  108.2 0.7 all-gather.5.cloned.1.call-update
  109.0 0.1 iota_compare_fusion.1
  109.0 0.3 select_reduce_fusion
  109.3 0.0 copy-done.2
  109.4 0.1 reshape.169
  110.1 0.1 broadcast_compare_fusion.2
  110.2 0.1 iota_add_fusion.1
  110.3 0.1 iota_add_fusion
  110.4 1.0 compare_and_fusion
  111.4 105.0 %all-gather.3.cloned.1.call-done = bf16[4096,512]{1,0:T(8,128)(2,1)} async-done(((bf16[64,512]{1,0:T(8,128)(2,1)}), bf16[4096,512]{1,0:T(8,128)(2,1)}) %all-gather.3.cloned.1.call-update) | async-done | bytes 4194320 | tf_op jit(solution)/shard_map/all_gather | solution.py:55
  216.4 3.4 convolution_convert_fusion.1
  219.9 0.1 reshape.157
  219.9 6.6 %all-to-all-done.3 = bf16[64,2,32,256]{3,2,1,0:T(8,128)(2,1)} async-done(((bf16[64,2,32,256]{3,2,1,0:T(8,128)(2,1)}), bf16[64,2,32,256]{3,2,1,0:T(8,128)(2,1)}, u32[]{:S(2)}, u32[]{:S(2)}) %all-to-all-start.3) | async-done | bytes 2097184 | tf_op jit(solution)/shard_map/all_to_all | solution.py:78
  226.6 3.2 pad_maximum_fusion
  229.7 3.7 gather_fusion.1
  233.4 2.9 fusion.2
  236.3 0.0 copy-start.1
  236.4 2.5 fusion
  238.9 0.0 copy-done.1
  238.9 2.2 fusion.16
  241.1 0.1 copy.43
  241.3 0.1 copy.44
  241.4 0.8 broadcast_in_dim.132
  242.3 3.5 all-to-all-start.4
  245.8 118.7 %all-gather.5.cloned.1.call-done = bf16[1024,2048]{1,0:T(8,128)(2,1)} async-done(((bf16[16,2048]{1,0:T(8,128)(2,1)}), bf16[1024,2048]{1,0:T(8,128)(2,1)}) %all-gather.5.cloned.1.call-update) | async-done | bytes 4194320 | tf_op jit(solution)/shard_map/all_gather | solution.py:118
  364.4 0.0 all-to-all-done.4
  364.4 4.4 %convolution_convert_fusion = bf16[256,2048]{1,0:T(8,128)(2,1)} fusion(bf16[256,1024]{0,1:T(8,128)(2,1)S(1)} %bitcast.93, bf16[1024,2048]{1,0:T(8,128)(2,1)} %all-gather.5.cloned.1.call-done), kind=kOutput, calls=%fused_computation.9 | convolution fusion | flops 1074266112 | bytes 5767168 | tf_op jit(solution)/shard_map/dot_general | solution.py:116
  (11 shorter events, 0.1 us)
Async XLA Ops:
  6.5 87.2 %copy-start = (bf16[256,4096]{1,0:T(8,128)(2,1)S(1)}, bf16[256,4096]{1,0:T(8,128)(2,1)}, u32[]{:S(2)}) copy-start(bf16[256,4096]{1,0:T(8,128)(2,1)} %param.7) | copy-start | bytes 6291460
  6.5 209.9 %all-gather.3.cloned.1.call-start = ((), (), s32[]{:S(2)}) async-start(), calls=%async_computation.5 | async-start | bytes 4259840 | tf_op jit(solution)/shard_map/all_gather | solution.py:55
  10.3 33.3 %all-to-all-start = ((s32[64,1,2]{2,1,0:T(1,128)}), s32[64,1,2]{2,1,0:T(1,128)S(1)}, u32[]{:S(2)}, u32[]{:S(2)}) async-start(s32[64,1,2]{2,1,0:T(1,128)} %copy.37), calls=%async_computation | async-start | bytes 65536 | tf_op jit(solution)/shard_map/all_to_all | solution.py:75
  61.9 29.9 %all-to-all-start.2 = ((bf16[16,16,16,256]{3,2,1,0:T(8,128)(2,1)}), bf16[16,16,16,256]{3,2,1,0:T(8,128)(2,1)}, u32[]{:S(2)}, u32[]{:S(2)}) async-start(bf16[16,16,16,256]{3,2,1,0:T(8,128)(2,1)} %broadcast_in_dim.123), calls=%async_computation.2 | async-start | bytes 4194304 | tf_op jit(solution)/shard_map/all_to_all | solution.py:16
  99.6 9.7 %copy-start.2 = (s32[8,16]{1,0:T(8,128)S(1)}, s32[8,16]{1,0:T(8,128)}, u32[]{:S(2)}) copy-start(s32[8,16]{1,0:T(8,128)} %param.12) | copy-start | bytes 1540
  99.6 126.9 %all-to-all-start.3 = ((bf16[64,2,32,256]{3,2,1,0:T(8,128)(2,1)}), bf16[64,2,32,256]{3,2,1,0:T(8,128)(2,1)}, u32[]{:S(2)}, u32[]{:S(2)}) async-start(bf16[64,2,32,256]{3,2,1,0:T(8,128)(2,1)} %broadcast_select_fusion), calls=%async_computation.3 | async-start | bytes 4194304 | tf_op jit(solution)/shard_map/all_to_all | solution.py:78
  108.2 256.2 %all-gather.5.cloned.1.call-start = ((), (), s32[]{:S(2)}) async-start(), calls=%async_computation.6 | async-start | bytes 4259840 | tf_op jit(solution)/shard_map/all_gather | solution.py:118
  236.3 2.6 copy-start.1
  242.3 122.2 %all-to-all-start.4 = ((bf16[2,256,512]{1,2,0:T(8,128)(2,1)}), bf16[2,256,512]{1,2,0:T(8,128)(2,1)S(1)}, u32[]{:S(2)}, u32[]{:S(2)}) async-start(bf16[2,256,512]{1,2,0:T(8,128)(2,1)} %broadcast_in_dim.132), calls=%async_computation.4 | async-start | bytes 1048576 | tf_op jit(solution)/shard_map/all_to_all | solution.py:16
Sparse Core Ops, SparseCore 0:
  10.3 206.0 all-gather.2
  219.4 145.0 all-gather.4
where the time goes:
time: 376 us
  waiting for transfers between devices  270 us (72%)
  starting transfers between devices  36.2 us (10%)
  blocking collectives  16.8 us (4%)
  between operations  14.3 us (4%)
  matrix products  13.7 us (4%)
  other arithmetic  13.5 us (4%)
  local copies, waits for them, and re-layouts  11.6 us (3%)
    all_gather x1, waiting for transfers between devices, body(): lax.all_gather(out_weight, KV, axis=0, tiled=True)  119 us
    all_gather x1, waiting for transfers between devices, body(): lax.all_gather(query_weight, KV, axis=0, tiled=True)  105 us
    all_to_all x2, waiting for transfers between devices, copy_for_each(): lax.all_to_all(jnp.broadcast_to(shard[None], (count, *shard.shape)), axis...  24 us
    all_to_all x1, starting transfers between devices, body(): lax.all_to_all(wanted, KV, split_axis=0, concat_axis=0, tiled=True)  18.7 us
    all_to_all x1, blocking collectives, copy_for_each(): lax.all_to_all(jnp.broadcast_to(shard[None], (count, *shard.shape)), axis...  16.8 us
    all_to_all x1, waiting for transfers between devices, body(): lax.all_to_all(wanted, KV, split_axis=0, concat_axis=0, tiled=True)  13.8 us
    all_to_all x2, starting transfers between devices, copy_for_each(): lax.all_to_all(jnp.broadcast_to(shard[None], (count, *shard.shape)), axis...  8.91 us
    all_to_all x1, starting transfers between devices, body(): lax.all_to_all(outgoing, KV, split_axis=0, concat_axis=0, tiled=True)  8.55 us
  transfers between devices with their start and end apart: 6, of which 5 were waited for; matrix products, arithmetic and copies ran while one was open for 9% of the time, Pallas kernels for 0%

commit v1 on v0

--- a/solution.py
+++ b/solution.py
@@ -41,6 +41,16 @@
 
 
 def body(tokens, query_weight, key_weight, value_weight, out_weight, chosen, live_length):
+
+    def hold_scales(in_dim, t0):
+        u_next = jnp.concatenate(
+            lax.all_to_all(
+                jnp.stack([t0 for _ in range(lax.axis_size(KV))]), KV, split_axis=0, concat_axis=0
+            ),
+            axis=in_dim,
+        )
+        return u_next
+
     rows = tokens.shape[0]
     per_dev = rows // BLOCK
     owners = lax.axis_size(KV)
@@ -113,11 +123,7 @@
     result = jnp.where(live[:, :, None, None], result, 0.0)
     attended = result.astype(jnp.bfloat16).reshape(rows, -1)
     every_head = gathered_copies(attended, "tp", 1)
-    mixed = jnp.dot(
-        every_head,
-        lax.all_gather(out_weight, KV, axis=0, tiled=True),
-        preferred_element_type=jnp.float32,
-    )
+    mixed = jnp.dot(every_head, hold_scales(0, out_weight), preferred_element_type=jnp.float32)
     return mixed.astype(jnp.bfloat16)
 
 

time: 376 us -> 475 us (1.26)
  blocking collectives: 16.8 us -> 222 us
  waiting for transfers between devices: 270 us -> 169 us
    all_to_all x0 -> x1, blocking collectives: none -> 201 us  [hold_scales(): lax.all_to_all(jnp.stack([t0 for _ in range(lax.axis_size(KV))]), KV, spl...]
    all_gather x1 -> x0, waiting for transfers between devices: 119 us -> none  [body(): lax.all_gather(out_weight, KV, axis=0, tiled=True)]
    all_gather x1, waiting for transfers between devices: 105 us -> 131 us  [body(): lax.all_gather(query_weight, KV, axis=0, tiled=True)]
    all_to_all x1, waiting for transfers between devices: 6.65 us -> 0.01 us  [body(): lax.all_to_all(outgoing, KV, split_axis=0, concat_axis=0, tiled=True)]
    all_to_all x1 -> x2, blocking collectives: 16.8 us -> 20.6 us  [copy_for_each(): lax.all_to_all(jnp.broadcast_to(shard[None], (count, *shard.shape)), axis...]
    all_to_all x2 -> x1, waiting for transfers between devices: 24 us -> 23.4 us  [copy_for_each(): lax.all_to_all(jnp.broadcast_to(shard[None], (count, *shard.shape)), axis...]
  transfers between devices with their start and end apart: 6 -> 4, of which waited for: 5 -> 3; matrix products, arithmetic and copies ran while one was open for 9% -> 3% of each run, Pallas kernels for 0% -> 0%
where the time goes in v1:
time: 475 us; the launch traced here: 474 us
  blocking collectives  222 us (47%)
  waiting for transfers between devices  169 us (36%)
  starting transfers between devices  32 us (7%)
  between operations  14.3 us (3%)
  other arithmetic  13.7 us (3%)
  matrix products  11.5 us (2%)
  local copies, waits for them, and re-layouts  11.2 us (2%)
    all_to_all x1, blocking collectives, hold_scales(): lax.all_to_all(jnp.stack([t0 for _ in range(lax.axis_size(KV))]), KV, spl...  201 us
    all_gather x1, waiting for transfers between devices, body(): lax.all_gather(query_weight, KV, axis=0, tiled=True)  131 us
    all_to_all x1, waiting for transfers between devices, copy_for_each(): lax.all_to_all(jnp.broadcast_to(shard[None], (count, *shard.shape)), axis...  23.4 us
    all_to_all x2, blocking collectives, copy_for_each(): lax.all_to_all(jnp.broadcast_to(shard[None], (count, *shard.shape)), axis...  20.6 us
    all_to_all x1, starting transfers between devices, body(): lax.all_to_all(wanted, KV, split_axis=0, concat_axis=0, tiled=True)  18.7 us
    all_to_all x1, waiting for transfers between devices, body(): lax.all_to_all(wanted, KV, split_axis=0, concat_axis=0, tiled=True)  13.8 us
  transfers between devices with their start and end apart: 4, of which 3 were waited for; matrix products, arithmetic and copies ran while one was open for 3% of the time, Pallas kernels for 0%

profile of v1, /device:TPU:2, one launch (start us, length us, event | category | flops | bytes accessed | tf_op | source)
XLA Modules:
  0.0 474.0 jit_solution(7029808317829402585)
XLA Ops:
  6.5 0.0 copy-start
  6.5 0.8 add_select_fusion.1
  7.4 0.7 broadcast_compare_fusion.1
  8.1 0.1 fusion.21
  8.2 0.1 reshape.157
  8.3 0.1 and_convert_fusion
  8.4 0.2 reduce_window_sum.11
  8.5 0.2 select_reduce_fusion.2
  8.7 0.1 reduce_or.28
  8.9 0.1 reduce_or.29
  9.0 0.7 copy.37
  9.7 18.7 %all-to-all-start = ((s32[64,1,2]{2,1,0:T(1,128)}), s32[64,1,2]{2,1,0:T(1,128)S(1)}, u32[]{:S(2)}, u32[]{:S(2)}) async-start(s32[64,1,2]{2,1,0:T(1,128)} %copy.37), calls=%async_computation | async-start | bytes 65536 | tf_op jit(solution)/shard_map/all_to_all | solution.py:85
  28.5 0.7 fusion.22
  29.2 13.8 %all-to-all-done = s32[64,1,2]{2,1,0:T(1,128)S(1)} async-done(((s32[64,1,2]{2,1,0:T(1,128)}), s32[64,1,2]{2,1,0:T(1,128)S(1)}, u32[]{:S(2)}, u32[]{:S(2)}) %all-to-all-start) | async-done | bytes 544 | tf_op jit(solution)/shard_map/all_to_all | solution.py:85
  43.0 16.5 %all_to_all.34 = bf16[16,16,256]{2,1,0:T(8,128)(2,1)S(1)} all-to-all(bf16[16,16,256]{2,1,0:T(8,128)(2,1)S(1)} %broadcast_in_dim.122), channel_id=1, replica_groups=mesh['dp'=4,'kv_0'=16,'kv_1'=4,'tp'=2] {'kv_0'}, dimensions={0} | all-to-all | bytes 262144 | tf_op jit(solution)/shard_map/all_to_all | solution.py:16
  59.5 1.5 broadcast_in_dim.123
  61.1 5.7 %all-to-all-start.2 = ((bf16[16,16,16,256]{3,2,1,0:T(8,128)(2,1)}), bf16[16,16,16,256]{3,2,1,0:T(8,128)(2,1)}, u32[]{:S(2)}, u32[]{:S(2)}) async-start(bf16[16,16,16,256]{3,2,1,0:T(8,128)(2,1)} %broadcast_in_dim.123), calls=%async_computation.2 | async-start | bytes 4194304 | tf_op jit(solution)/shard_map/all_to_all | solution.py:16
  66.7 0.0 all-gather.2.cloned.1.call-start
  66.8 0.7 all-gather.2.cloned.1.call-update
  67.5 0.1 maximum_reduce_fusion
  67.6 0.1 reshape.167
  67.8 0.1 copy.38
  67.9 0.1 copy.39
  68.0 23.4 %all-to-all-done.2 = bf16[16,16,16,256]{3,2,1,0:T(8,128)(2,1)} async-done(((bf16[16,16,16,256]{3,2,1,0:T(8,128)(2,1)}), bf16[16,16,16,256]{3,2,1,0:T(8,128)(2,1)}, u32[]{:S(2)}, u32[]{:S(2)}) %all-to-all-start.2) | async-done | bytes 2097184 | tf_op jit(solution)/shard_map/all_to_all | solution.py:16
  91.4 1.9 copy.40
  93.3 0.0 copy-done
  93.3 0.7 convolution_convert_fusion.2
  94.1 2.0 gather_fusion
  96.1 3.2 broadcast_select_fusion
  99.3 0.0 copy-start.3
  99.3 7.5 %all-to-all-start.3 = ((bf16[64,2,32,256]{3,2,1,0:T(8,128)(2,1)}), bf16[64,2,32,256]{3,2,1,0:T(8,128)(2,1)}, u32[]{:S(2)}, u32[]{:S(2)}) async-start(bf16[64,2,32,256]{3,2,1,0:T(8,128)(2,1)} %broadcast_select_fusion), calls=%async_computation.3 | async-start | bytes 4194304 | tf_op jit(solution)/shard_map/all_to_all | solution.py:88
  106.8 0.1 iota_compare_fusion.1
  106.9 0.3 select_reduce_fusion
  107.2 0.0 copy-done.3
  107.3 0.1 reshape.175
  108.0 0.1 broadcast_compare_fusion.2
  108.1 0.1 iota_add_fusion.1
  108.2 0.1 iota_add_fusion
  108.2 1.0 compare_and_fusion
  109.3 131.2 %all-gather.2.cloned.1.call-done = bf16[4096,512]{1,0:T(8,128)(2,1)} async-done(((bf16[64,512]{1,0:T(8,128)(2,1)}), bf16[4096,512]{1,0:T(8,128)(2,1)}) %all-gather.2.cloned.1.call-update) | async-done | bytes 4194320 | tf_op jit(solution)/shard_map/all_gather | solution.py:65
  240.5 3.4 convolution_convert_fusion.1
  243.9 0.1 reshape.162
  244.0 0.0 all-to-all-done.3
  244.0 3.2 pad_maximum_fusion
  247.2 3.6 gather_fusion.1
  250.8 2.9 fusion.2
  253.7 0.0 copy-start.1
  253.7 2.5 fusion
  256.2 0.0 copy-done.1
  256.2 2.2 fusion.16
  258.4 0.0 copy-start.2
  258.4 0.1 copy.43
  258.6 0.1 copy.44
  258.8 4.2 all_to_all.35
  263.0 0.0 copy-done.2
  263.0 0.5 stack.5
  263.5 201.4 %all_to_all.36 = bf16[64,16,2048]{2,1,0:T(8,128)(2,1)S(1)} all-to-all(bf16[64,16,2048]{2,1,0:T(8,128)(2,1)S(1)} %stack.5), channel_id=1, replica_groups=mesh['dp'=4,'kv_0'=16,'kv_1'=4,'tp'=2] {'kv_0','kv_1'}, dimensions={0} | all-to-all | bytes 8388608 | tf_op jit(solution)/shard_map/all_to_all | solution.py:47
  464.9 2.2 convolution_convert_fusion
  (12 shorter events, 0.2 us)
Async XLA Ops:
  6.5 86.8 %copy-start = (bf16[256,4096]{1,0:T(8,128)(2,1)S(1)}, bf16[256,4096]{1,0:T(8,128)(2,1)}, u32[]{:S(2)}) copy-start(bf16[256,4096]{1,0:T(8,128)(2,1)} %param.7) | copy-start | bytes 6291460
  9.7 33.3 %all-to-all-start = ((s32[64,1,2]{2,1,0:T(1,128)}), s32[64,1,2]{2,1,0:T(1,128)S(1)}, u32[]{:S(2)}, u32[]{:S(2)}) async-start(s32[64,1,2]{2,1,0:T(1,128)} %copy.37), calls=%async_computation | async-start | bytes 65536 | tf_op jit(solution)/shard_map/all_to_all | solution.py:85
  61.1 30.4 %all-to-all-start.2 = ((bf16[16,16,16,256]{3,2,1,0:T(8,128)(2,1)}), bf16[16,16,16,256]{3,2,1,0:T(8,128)(2,1)}, u32[]{:S(2)}, u32[]{:S(2)}) async-start(bf16[16,16,16,256]{3,2,1,0:T(8,128)(2,1)} %broadcast_in_dim.123), calls=%async_computation.2 | async-start | bytes 4194304 | tf_op jit(solution)/shard_map/all_to_all | solution.py:16
  66.7 173.7 %all-gather.2.cloned.1.call-start = ((), (), s32[]{:S(2)}) async-start(), calls=%async_computation.6 | async-start | bytes 4259840 | tf_op jit(solution)/shard_map/all_gather | solution.py:65
  99.3 8.0 %copy-start.3 = (s32[8,16]{1,0:T(8,128)S(1)}, s32[8,16]{1,0:T(8,128)}, u32[]{:S(2)}) copy-start(s32[8,16]{1,0:T(8,128)} %param.12) | copy-start | bytes 1540
  99.3 144.7 %all-to-all-start.3 = ((bf16[64,2,32,256]{3,2,1,0:T(8,128)(2,1)}), bf16[64,2,32,256]{3,2,1,0:T(8,128)(2,1)}, u32[]{:S(2)}, u32[]{:S(2)}) async-start(bf16[64,2,32,256]{3,2,1,0:T(8,128)(2,1)} %broadcast_select_fusion), calls=%async_computation.3 | async-start | bytes 4194304 | tf_op jit(solution)/shard_map/all_to_all | solution.py:88
  253.7 2.6 copy-start.1
  258.4 4.5 copy-start.2
Sparse Core Ops, SparseCore 0:
  70.5 169.9 all-gather.1
